TPU v7x, 512 devices: a 4x2x32 block of a 4x8x32 slice. The times are simulated.
512 devices in a mesh: grp: 2 (over y), ep: 64 (over z, core), tp: 4 (over x).
Axes of the slice: x: 4, y: 2, z: 32, core: 2. Of those that a mesh axis runs over, the one named last changes fastest.
The devices are a block of a 4x8x32 slice.
Arguments:
- tokens: bfloat16 [49152, 2048], P(('grp', 'ep'), 'tp'), parts along dimension 0
- group_choice: int32 [49152], P(('grp', 'ep')), parts along dimension 0, may hold values from 0 to 7, as said below
- expert_choice: int32 [49152, 2], P(('grp', 'ep')), parts along dimension 0, may hold values from 0 to 7, as said below
- group_weight: float32 [49152], P(('grp', 'ep')), parts along dimension 0, may hold values from 0.3 to 1
- expert_weight: float32 [49152, 2], P(('grp', 'ep')), parts along dimension 0, may hold values from 0.1 to 1
- norm_gain: float32 [2048], replicated, may hold values from 0.1 to 1.9
- w_gate: bfloat16 [64, 2048, 1024], P('ep', None, 'tp'), may hold values from -0.125 to 0.125
- w_up: bfloat16 [64, 2048, 1024], P('ep', None, 'tp'), may hold values from -0.125 to 0.125
- w_down: bfloat16 [64, 1024, 2048], P('ep', None, 'tp'), may hold values from -0.1875 to 0.1875
Outputs:
- moe_out: bfloat16 [49152, 2048], P(('grp', 'ep'), 'tp'), parts along dimension 0
There are 2 independent parts, one for each index of `grp`. A program takes and returns all parts, laid end to end along the dimension named above; an argument that names none is the same for every part. Nothing has to cross between parts.
Inputs may be any that keep to these rules, and one draw needn't show every extreme that they name: `group_choice`: group of each token, 0 to 7; within each aligned block of 384 tokens (the tokens of one index of ep) every group is chosen by the same number of tokens. `expert_choice`: a token's two entries differ; within each aligned block of 384 tokens no expert (group with entry) is named by more than 18 tokens, and in every block one expert of each group, the same one in all blocks, is named by exactly 18 tokens.
All inputs are finite; a program needn't handle non-finite values.
Results may differ from a plain program's by a relative error of at most 0.0071.
Values may be sent and summed in bfloat16 or wider, within the bound.
A program may use at most 64 MiB of HBM per device.

v0:
```python
import jax
import jax.numpy as jnp
from jax import lax
from jax.sharding import Mesh
from jax.sharding import PartitionSpec as P

GRP_EP = ("grp", "g", "e")
EP = ("g", "e")
GROUP_SIZE = 8


def rank_before(marks):
    return jnp.cumsum(marks, -2) - marks


def body(
    tokens,
    group_choice,
    expert_choice,
    group_weight,
    expert_weight,
    norm_gain,
    w_gate,
    w_up,
    w_down,
):
    rows, width = tokens.shape
    groups = lax.axis_size("g")
    members = lax.axis_size("e")
    per_group = rows // groups
    mean_load = 2 * per_group // members
    capacity = mean_load + min(mean_load // 2, per_group - mean_load)
    model_width = norm_gain.shape[0]
    mixing = group_weight[:, None] * expert_weight / jnp.sum(expert_weight, -1, keepdims=True)
    group_marks = (group_choice[:, None] == jnp.arange(groups, dtype=jnp.int32)).astype(jnp.int32)
    place = group_choice * per_group + jnp.sum(rank_before(group_marks) * group_marks, 1)
    spots = jnp.arange(rows, dtype=jnp.int32)
    sort = spots[:, None] == place[None, :]
    values = tokens.astype(jnp.float32)
    squares = lax.all_gather(jnp.sum(values * values, -1), "tp", axis=0)
    inv_rms = lax.rsqrt(jnp.sum(squares, 0) / model_width + 1e-06)
    gain = lax.dynamic_slice_in_dim(norm_gain, lax.axis_index("tp") * width, width, 0)
    normed = (values * inv_rms[:, None] * gain[None, :]).astype(jnp.bfloat16)
    by_group = jnp.dot(
        sort.astype(jnp.bfloat16), normed, preferred_element_type=jnp.float32
    ).astype(jnp.bfloat16)
    facts = jnp.concatenate([expert_choice.astype(jnp.float32), mixing], -1)
    facts = jnp.dot(sort.astype(jnp.float32), facts, precision=lax.Precision.HIGHEST)
    landed = lax.all_to_all(
        by_group.reshape(groups, per_group, width), "g", 0, 0, tiled=True
    ).reshape(rows, width)
    facts = lax.all_to_all(facts.reshape(groups, per_group, 4), "g", 0, 0, tiled=True).reshape(
        rows, 4
    )
    chosen = facts[:, :2].astype(jnp.int32).reshape(groups, per_group, 2)
    blocks = jnp.arange(groups, dtype=jnp.int32)[:, None, None]
    kinds = jnp.arange(members, dtype=jnp.int32)
    marks = jnp.sum((chosen[..., None] == kinds).astype(jnp.int32), 2)
    ranks = rank_before(marks)
    seats = jnp.sum(jnp.where(chosen[..., None] == kinds, ranks[:, :, None, :], 0), -1)
    targets = (chosen * groups + blocks) * capacity + seats
    targets = targets.reshape(rows, 2)
    seats_all = members * groups * capacity
    places = jnp.arange(seats_all, dtype=jnp.int32)
    picks = [targets[None, :, k] == places[:, None] for k in range(2)]
    dispatch = (picks[0] | picks[1]).astype(jnp.bfloat16)
    buffer = jnp.dot(dispatch, landed, preferred_element_type=jnp.float32).astype(jnp.bfloat16)
    received = lax.all_to_all(
        buffer.reshape(members, groups * capacity, width), "e", 0, 0, tiled=True
    ).reshape(seats_all, width)
    piece = lax.all_gather(received, "tp", axis=1, tiled=True)
    gate = jnp.dot(piece, w_gate[0], preferred_element_type=jnp.float32)
    up = jnp.dot(piece, w_up[0], preferred_element_type=jnp.float32)
    hidden = (jax.nn.silu(gate) * up).astype(jnp.bfloat16)
    hidden = lax.all_gather(hidden, "tp", axis=1, tiled=True)
    result = jnp.dot(hidden, w_down[0], preferred_element_type=jnp.float32).astype(jnp.bfloat16)
    back = lax.all_to_all(
        result.reshape(members, groups * capacity, width), "e", 0, 0, tiled=True
    ).reshape(seats_all, width)
    mixed = jnp.zeros((rows, width), jnp.float32)
    for k in range(2):
        picker = (targets[:, k : k + 1] == places[None, :]).astype(jnp.bfloat16)
        picked = jnp.dot(picker, back, preferred_element_type=jnp.float32)
        mixed = mixed + facts[:, 2 + k : 3 + k] * picked
    home = lax.all_to_all(
        mixed.astype(jnp.bfloat16).reshape(groups, per_group, width), "g", 0, 0, tiled=True
    ).reshape(rows, width)
    unsort = place[:, None] == spots[None, :]
    return jnp.dot(unsort.astype(jnp.bfloat16), home, preferred_element_type=jnp.float32).astype(
        jnp.bfloat16
    )


def solution(mesh):
    members = GROUP_SIZE
    split = Mesh(
        mesh.devices.reshape(
            mesh.shape["grp"], mesh.shape["ep"] // members, members, mesh.shape["tp"]
        ),
        ("grp", "g", "e", "tp"),
    )
    placed = (
        P(GRP_EP, "tp"),
        P(GRP_EP),
        P(GRP_EP, None),
        P(GRP_EP),
        P(GRP_EP, None),
        P(),
        P(EP, None, "tp"),
        P(EP, None, "tp"),
        P(EP, None, "tp"),
    )
    return jax.shard_map(
        body, mesh=split, in_specs=placed, out_specs=P(GRP_EP, "tp"), check_vma=False
    )
```

profile of v0, /device:TPU:96, one launch (start us, length us, event | category | flops | bytes accessed | tf_op | source)
XLA Modules:
  0.0 404.2 jit_solution(10690738187043938088)
XLA Ops:
  6.6 0.8 convert_element_type.48
  7.3 0.7 fusion.29
  8.0 0.8 reduce-window.6
  8.9 0.2 slice_reduce_fusion
  9.1 0.8 fusion.28
  9.9 0.7 multiply_add_fusion.1
  10.6 0.7 reduce_sum.57
  11.3 0.7 multiply_divide_fusion
  12.0 0.4 fusion.20
  12.4 0.1 reshape.73
  12.5 0.7 reshape.92
  13.2 42.5 %all-to-all-start = ((f32[8,1,192]{2,1,0:T(1,128)}), f32[8,1,192]{2,1,0:T(1,128)S(1)}, u32[]{:S(2)}, u32[]{:S(2)}) async-start(f32[8,1,192]{2,1,0:T(1,128)} %reshape.92), calls=%async_computation | async-start | bytes 16384 | tf_op jit(solution)/shard_map/all_to_all | solution.py:52
  55.7 1.2 fusion.17
  56.9 11.4 %all-gather.1 = f32[4,1,384]{2,1,0:T(1,128)S(1)} all-gather(f32[1,1,384]{2,1,0:T(1,128)S(1)} %reshape.84), channel_id=2, replica_groups=mesh['grp'=2,'g'=8,'e'=8,'tp'=4] {'tp'}, dimensions={0}, use_global_device_ids=true | all-gather | bytes 7680 | tf_op jit(solution)/shard_map/all_gather | solution.py:40
  68.3 0.8 dynamic_slice.3
  69.1 2.2 convolution_convert_fusion.3
  71.3 6.7 %all-to-all-done = f32[8,1,192]{2,1,0:T(1,128)S(1)} async-done(((f32[8,1,192]{2,1,0:T(1,128)}), f32[8,1,192]{2,1,0:T(1,128)S(1)}, u32[]{:S(2)}, u32[]{:S(2)}) %all-to-all-start) | async-done | bytes 6176 | tf_op jit(solution)/shard_map/all_to_all | solution.py:52
  78.0 15.0 %all-to-all-start.1 = ((bf16[8,48,512]{2,1,0:T(8,128)(2,1)}), bf16[8,48,512]{2,1,0:T(8,128)(2,1)S(1)}, u32[]{:S(2)}, u32[]{:S(2)}) async-start(bf16[8,48,512]{2,1,0:T(8,128)(2,1)} %bitcast.3), calls=%async_computation.1 | async-start | bytes 786432 | tf_op jit(solution)/shard_map/all_to_all | solution.py:49
  92.9 0.1 all-gather.5.cloned.1.call-start
  93.0 0.1 add.42
  93.1 0.6 broadcast.44
  93.7 0.7 reduce.11
  94.4 0.1 reshape.93
  94.5 0.1 reshape.74
  94.6 0.1 eq.140
  94.7 0.1 copy.29
  94.8 3.8 reduce-window_subtract_fusion
  98.6 0.1 copy.31
  98.8 0.1 reduce_sum.60
  98.9 34.6 %all-to-all-done.1 = bf16[8,48,512]{2,1,0:T(8,128)(2,1)S(1)} async-done(((bf16[8,48,512]{2,1,0:T(8,128)(2,1)}), bf16[8,48,512]{2,1,0:T(8,128)(2,1)S(1)}, u32[]{:S(2)}, u32[]{:S(2)}) %all-to-all-start.1) | async-done | bytes 393248 | tf_op jit(solution)/shard_map/all_to_all | solution.py:49
  133.6 0.8 convolution_convert_fusion.1
  134.4 40.5 %all_to_all.25 = bf16[8,144,512]{2,1,0:T(8,128)(2,1)} all-to-all(bf16[8,144,512]{2,1,0:T(8,128)(2,1)S(1)} %bitcast.50), channel_id=1, replica_groups=mesh['grp'=2,'g'=8,'e'=8,'tp'=4] {'e'}, dimensions={0} | all-to-all | bytes 2359296 | tf_op jit(solution)/shard_map/all_to_all | solution.py:68
  174.9 0.1 all-gather.5.cloned.1.call-update
  174.9 0.0 copy-start.3
  175.0 0.1 all-gather.7.cloned.1.call-start
  175.0 52.6 %all-gather.5.cloned.1.call-done = bf16[1152,2048]{1,0:T(8,128)(2,1)} async-done(((bf16[1152,512]{1,0:T(8,128)(2,1)}), bf16[1152,2048]{1,0:T(8,128)(2,1)}) %all-gather.5.cloned.1.call-update) | async-done | bytes 4718608 | tf_op jit(solution)/shard_map/all_gather | solution.py:71
  227.7 3.9 fusion.11
  231.6 2.4 fusion
  234.0 0.1 all-gather.7.cloned.1.call-update
  234.0 53.1 %all-gather.7.cloned.1.call-done = bf16[1152,1024]{1,0:T(8,128)(2,1)} async-done(((bf16[1152,256]{1,0:T(8,128)(2,1)}), bf16[1152,1024]{1,0:T(8,128)(2,1)}) %all-gather.7.cloned.1.call-update) | async-done | bytes 2359312 | tf_op jit(solution)/shard_map/all_gather | solution.py:75
  287.2 0.0 copy-done
  287.2 4.1 %convolution_convert_fusion = bf16[1152,512]{1,0:T(8,128)(2,1)} fusion(bf16[1152,1024]{1,0:T(8,128)(2,1)} %all-gather.7.cloned.1.call-done, bf16[1,1024,512]{2,1,0:T(8,128)(2,1)S(1)} %copy-done), kind=kOutput, calls=%fused_computation | convolution fusion | flops 1208549376 | bytes 4587520 | tf_op jit(solution)/shard_map/dot_general | solution.py:76
  291.2 5.3 %all-to-all-start.3 = ((bf16[8,144,512]{2,1,0:T(8,128)(2,1)}), bf16[8,144,512]{2,1,0:T(8,128)(2,1)S(1)}, u32[]{:S(2)}, u32[]{:S(2)}) async-start(bf16[8,144,512]{2,1,0:T(8,128)(2,1)} %bitcast.10), calls=%async_computation.3 | async-start | bytes 2359296 | tf_op jit(solution)/shard_map/all_to_all | solution.py:77
  296.5 25.9 %all-to-all-done.3 = bf16[8,144,512]{2,1,0:T(8,128)(2,1)S(1)} async-done(((bf16[8,144,512]{2,1,0:T(8,128)(2,1)}), bf16[8,144,512]{2,1,0:T(8,128)(2,1)S(1)}, u32[]{:S(2)}, u32[]{:S(2)}) %all-to-all-start.3) | async-done | bytes 1179680 | tf_op jit(solution)/shard_map/all_to_all | solution.py:77
  322.4 0.7 fusion.7
  323.2 0.7 fusion.8
  323.9 72.3 %all_to_all.26 = bf16[8,48,512]{2,1,0:T(8,128)(2,1)S(1)} all-to-all(bf16[8,48,512]{2,1,0:T(8,128)(2,1)S(1)} %bitcast.52), channel_id=1, replica_groups=mesh['grp'=2,'g'=8,'e'=8,'tp'=4] {'g'}, dimensions={0} | all-to-all | bytes 786432 | tf_op jit(solution)/shard_map/all_to_all | solution.py:85
  396.2 1.2 convolution_convert_fusion.2
  (21 shorter events, 0.3 us)
Async XLA Ops:
  6.5 280.6 %copy-start = (bf16[1,1024,512]{2,1,0:T(8,128)(2,1)S(1)}, bf16[1,1024,512]{2,1,0:T(8,128)(2,1)}, u32[]{:S(2)}) copy-start(bf16[1,1024,512]{2,1,0:T(8,128)(2,1)} %param.17) | copy-start | bytes 3145732
  13.2 64.8 %all-to-all-start = ((f32[8,1,192]{2,1,0:T(1,128)}), f32[8,1,192]{2,1,0:T(1,128)S(1)}, u32[]{:S(2)}, u32[]{:S(2)}) async-start(f32[8,1,192]{2,1,0:T(1,128)} %reshape.92), calls=%async_computation | async-start | bytes 16384 | tf_op jit(solution)/shard_map/all_to_all | solution.py:52
  78.0 55.6 %all-to-all-start.1 = ((bf16[8,48,512]{2,1,0:T(8,128)(2,1)}), bf16[8,48,512]{2,1,0:T(8,128)(2,1)S(1)}, u32[]{:S(2)}, u32[]{:S(2)}) async-start(bf16[8,48,512]{2,1,0:T(8,128)(2,1)} %bitcast.3), calls=%async_computation.1 | async-start | bytes 786432 | tf_op jit(solution)/shard_map/all_to_all | solution.py:49
  92.9 134.7 %all-gather.5.cloned.1.call-start = ((), (), s32[]{:S(2)}) async-start(), calls=%async_computation.5 | async-start | bytes 5898240 | tf_op jit(solution)/shard_map/all_gather | solution.py:71
  174.9 52.8 %copy-start.2 = (bf16[1,2048,256]{2,1,0:T(8,128)(2,1)S(1)}, bf16[1,2048,256]{2,1,0:T(8,128)(2,1)}, u32[]{:S(2)}) copy-start(bf16[1,2048,256]{2,1,0:T(8,128)(2,1)} %param.15) | copy-start | bytes 3145732
  174.9 56.6 %copy-start.3 = (bf16[1,2048,256]{2,1,0:T(8,128)(2,1)S(1)}, bf16[1,2048,256]{2,1,0:T(8,128)(2,1)}, u32[]{:S(2)}) copy-start(bf16[1,2048,256]{2,1,0:T(8,128)(2,1)} %param.16) | copy-start | bytes 3145732
  175.0 112.2 %all-gather.7.cloned.1.call-start = ((), (), s32[]{:S(2)}) async-start(), calls=%async_computation.6 | async-start | bytes 2949120 | tf_op jit(solution)/shard_map/all_gather | solution.py:75
  227.7 3.9 copy-start.1
  291.2 31.2 %all-to-all-start.3 = ((bf16[8,144,512]{2,1,0:T(8,128)(2,1)}), bf16[8,144,512]{2,1,0:T(8,128)(2,1)S(1)}, u32[]{:S(2)}, u32[]{:S(2)}) async-start(bf16[8,144,512]{2,1,0:T(8,128)(2,1)} %bitcast.10), calls=%async_computation.3 | async-start | bytes 2359296 | tf_op jit(solution)/shard_map/all_to_all | solution.py:77
Sparse Core Ops, SparseCore 0:
  175.1 52.5 all-gather.4
  234.1 52.9 all-gather.6
where the time goes:
time: 405 us; the launch traced here: 404 us
  waiting for transfers between devices  173 us (43%)
  blocking collectives  124 us (31%)
  starting transfers between devices  62.9 us (16%)
  matrix products  16.3 us (4%)
  between operations  13.6 us (3%)
  other arithmetic  11 us (3%)
    all_to_all x1, blocking collectives, body(): lax.all_to_all(mixed.astype(jnp.bfloat16).reshape(groups, per_group, widt...  72.3 us
    all_gather x1, waiting for transfers between devices, body(): hidden = lax.all_gather(hidden, 'tp', axis=1, tiled=True)  53.1 us
    all_gather x1, waiting for transfers between devices, body(): piece = lax.all_gather(received, 'tp', axis=1, tiled=True)  52.6 us
    all_to_all x1, starting transfers between devices, body(): lax.all_to_all(facts.reshape(groups, per_group, 4), 'g', 0, 0, tiled=True)  42.5 us
    all_to_all x1, blocking collectives, body(): lax.all_to_all(buffer.reshape(members, groups * capacity, width), 'e', 0,...  40.5 us
    all_to_all x1, waiting for transfers between devices, body(): lax.all_to_all(by_group.reshape(groups, per_group, width), 'g', 0, 0, til...  34.6 us
    all_to_all x1, waiting for transfers between devices, body(): lax.all_to_all(result.reshape(members, groups * capacity, width), 'e', 0,...  25.9 us
    all_to_all x1, starting transfers between devices, body(): lax.all_to_all(by_group.reshape(groups, per_group, width), 'g', 0, 0, til...  15 us
  transfers between devices with their start and end apart: 5, of which 5 were waited for; matrix products, arithmetic and copies ran while one was open for 2% of the time, Pallas kernels for 0%

commit v1 on v0

--- a/solution.py
+++ b/solution.py
@@ -7,6 +7,35 @@
 GRP_EP = ("grp", "g", "e")
 EP = ("g", "e")
 GROUP_SIZE = 8
+
+
+def _enter_sections(inp, in_dim):
+    known = list(inp.shape[1:])
+    known[in_dim] *= inp.shape[0]
+    return jnp.moveaxis(inp, 0, in_dim).reshape(known)
+
+
+def series_deliver(here_x, a_name, along_dim):
+    count_all = lax.axis_size(a_name)
+    pile = [(dd, (dd + 1) % count_all) for dd in range(count_all)]
+    column = [(to_i, at) for at, to_i in pile]
+    k_now, mid_arr = ([], [])
+    for s in [*range(count_all - 1)]:
+        if s % 2 == 0:
+            current_value = lax.ppermute(
+                k_now[-1] if k_now else here_x, axis_name=a_name, perm=pile
+            )
+            k_now.append(current_value)
+        else:
+            side_arr = lax.ppermute(
+                mid_arr[-1] if mid_arr else here_x, axis_name=a_name, perm=column
+            )
+            mid_arr.append(side_arr)
+    local_out = jnp.stack([*k_now[::-1], here_x, *mid_arr], 0)
+    built = lax.axis_index(a_name)
+    shaped = built - len(k_now)
+    local_out = local_out[(jnp.arange(count_all) - shaped) % count_all]
+    return _enter_sections(local_out, along_dim)
 
 
 def rank_before(marks):
@@ -72,7 +101,7 @@
     gate = jnp.dot(piece, w_gate[0], preferred_element_type=jnp.float32)
     up = jnp.dot(piece, w_up[0], preferred_element_type=jnp.float32)
     hidden = (jax.nn.silu(gate) * up).astype(jnp.bfloat16)
-    hidden = lax.all_gather(hidden, "tp", axis=1, tiled=True)
+    hidden = series_deliver(hidden, "tp", 1)
     result = jnp.dot(hidden, w_down[0], preferred_element_type=jnp.float32).astype(jnp.bfloat16)
     back = lax.all_to_all(
         result.reshape(members, groups * capacity, width), "e", 0, 0, tiled=True

time: 405 us -> 393 us (0.970)
  waiting for transfers between devices: 173 us -> 146 us
  starting transfers between devices: 62.9 us -> 71.9 us
  local copies, waits for them, and re-layouts: 3.1 us -> 9.05 us
    all_gather x1 -> x0, waiting for transfers between devices: 53.1 us -> none  [body(): hidden = lax.all_gather(hidden, 'tp', axis=1, tiled=True)]
    ppermute x0 -> x3, waiting for transfers between devices: none -> 26.1 us  [the longest x2 26.1 us: series_deliver(): lax.ppermute(k_now[-1] if k_now else here_x, axis_name=a_name, perm=pile)]
    ppermute x0 -> x3, starting transfers between devices: none -> 9.05 us  [the longest x2 4.8 us: series_deliver(): lax.ppermute(k_now[-1] if k_now else here_x, axis_name=a_name, perm=pile)]
  transfers between devices with their start and end apart: 5 -> 7, of which waited for: 5 -> 6; matrix products, arithmetic and copies ran while one was open for 2% -> 3% of each run, Pallas kernels for 0% -> 0%
where the time goes in v1:
time: 393 us; the launch traced here: 392 us
  waiting for transfers between devices  146 us (37%)
  blocking collectives  124 us (32%)
  starting transfers between devices  71.9 us (18%)
  matrix products  13.9 us (4%)
  between operations  13.7 us (3%)
  other arithmetic  12.9 us (3%)
  local copies, waits for them, and re-layouts  9.05 us (2%)
    all_to_all x1, blocking collectives, body(): lax.all_to_all(mixed.astype(jnp.bfloat16).reshape(groups, per_group, widt...  72.3 us
    all_gather x1, waiting for transfers between devices, body(): piece = lax.all_gather(received, 'tp', axis=1, tiled=True)  52.6 us
    all_to_all x1, starting transfers between devices, body(): lax.all_to_all(facts.reshape(groups, per_group, 4), 'g', 0, 0, tiled=True)  42.5 us
    all_to_all x1, blocking collectives, body(): lax.all_to_all(buffer.reshape(members, groups * capacity, width), 'e', 0,...  40.7 us
    all_to_all x1, waiting for transfers between devices, body(): lax.all_to_all(by_group.reshape(groups, per_group, width), 'g', 0, 0, til...  34.6 us
    ppermute x2, waiting for transfers between devices, series_deliver(): lax.ppermute(k_now[-1] if k_now else here_x, axis_name=a_name, perm=pile)  26.1 us
    all_to_all x1, waiting for transfers between devices, body(): lax.all_to_all(result.reshape(members, groups * capacity, width), 'e', 0,...  25.9 us
    all_to_all x1, starting transfers between devices, body(): lax.all_to_all(by_group.reshape(groups, per_group, width), 'g', 0, 0, til...  15 us
  transfers between devices with their start and end apart: 7, of which 6 were waited for; matrix products, arithmetic and copies ran while one was open for 3% of the time, Pallas kernels for 0%

profile of v1, /device:TPU:96, one launch (start us, length us, event | category | flops | bytes accessed | tf_op | source)
XLA Modules:
  0.0 391.8 jit_solution(7656945858088602799)
XLA Ops:
  6.6 0.8 fusion.29
  7.3 0.8 reduce-window.6
  8.2 0.2 slice_reduce_fusion
  8.4 0.8 fusion.28
  9.2 0.7 multiply_add_fusion.1
  9.9 0.7 convert_element_type.48
  10.6 0.7 reduce_sum.57
  11.3 0.7 multiply_divide_fusion
  12.0 0.4 fusion.20
  12.4 0.1 reshape.125
  12.5 0.7 reshape.153
  13.2 42.5 %all-to-all-start = ((f32[8,1,192]{2,1,0:T(1,128)}), f32[8,1,192]{2,1,0:T(1,128)S(1)}, u32[]{:S(2)}, u32[]{:S(2)}) async-start(f32[8,1,192]{2,1,0:T(1,128)} %reshape.153), calls=%async_computation | async-start | bytes 16384 | tf_op jit(solution)/shard_map/all_to_all | solution.py:81
  55.7 1.2 fusion.17
  56.9 11.4 %all-gather.1 = f32[4,1,384]{2,1,0:T(1,128)S(1)} all-gather(f32[1,1,384]{2,1,0:T(1,128)S(1)} %reshape.145), channel_id=2, replica_groups=mesh['grp'=2,'g'=8,'e'=8,'tp'=4] {'tp'}, dimensions={0}, use_global_device_ids=true | all-gather | bytes 7680 | tf_op jit(solution)/shard_map/all_gather | solution.py:69
  68.3 0.8 dynamic_slice.3
  69.1 2.2 convolution_convert_fusion.3
  71.3 6.7 %all-to-all-done = f32[8,1,192]{2,1,0:T(1,128)S(1)} async-done(((f32[8,1,192]{2,1,0:T(1,128)}), f32[8,1,192]{2,1,0:T(1,128)S(1)}, u32[]{:S(2)}, u32[]{:S(2)}) %all-to-all-start) | async-done | bytes 6176 | tf_op jit(solution)/shard_map/all_to_all | solution.py:81
  77.9 15.0 %all-to-all-start.1 = ((bf16[8,48,512]{2,1,0:T(8,128)(2,1)}), bf16[8,48,512]{2,1,0:T(8,128)(2,1)S(1)}, u32[]{:S(2)}, u32[]{:S(2)}) async-start(bf16[8,48,512]{2,1,0:T(8,128)(2,1)} %bitcast.3), calls=%async_computation.1 | async-start | bytes 786432 | tf_op jit(solution)/shard_map/all_to_all | solution.py:78
  93.1 0.6 broadcast.113
  93.7 0.7 reduce.11
  94.5 0.1 reshape.126
  94.6 0.1 eq.142
  94.7 0.1 copy.33
  94.8 3.8 reduce-window_subtract_fusion
  98.6 0.1 copy.35
  98.8 0.1 reduce_sum.60
  98.9 34.6 %all-to-all-done.1 = bf16[8,48,512]{2,1,0:T(8,128)(2,1)S(1)} async-done(((bf16[8,48,512]{2,1,0:T(8,128)(2,1)}), bf16[8,48,512]{2,1,0:T(8,128)(2,1)S(1)}, u32[]{:S(2)}, u32[]{:S(2)}) %all-to-all-start.1) | async-done | bytes 393248 | tf_op jit(solution)/shard_map/all_to_all | solution.py:78
  133.6 0.8 convolution_convert_fusion.1
  134.4 40.7 %all_to_all.25 = bf16[8,144,512]{2,1,0:T(8,128)(2,1)} all-to-all(bf16[8,144,512]{2,1,0:T(8,128)(2,1)S(1)} %bitcast.61), channel_id=1, replica_groups=mesh['grp'=2,'g'=8,'e'=8,'tp'=4] {'e'}, dimensions={0} | all-to-all | bytes 2359296 | tf_op jit(solution)/shard_map/all_to_all | solution.py:97
  175.1 52.6 %all-gather.4.cloned.1.call-done = bf16[1152,2048]{1,0:T(8,128)(2,1)} async-done(((bf16[1152,512]{1,0:T(8,128)(2,1)}), bf16[1152,2048]{1,0:T(8,128)(2,1)}) %all-gather.4.cloned.1.call-update) | async-done | bytes 4718608 | tf_op jit(solution)/shard_map/all_gather | solution.py:100
  227.8 3.9 fusion.11
  231.7 1.6 fusion
  233.2 2.9 collective-permute-start
  236.1 4.2 %collective-permute-start.2 = (bf16[1152,256]{1,0:T(8,128)(2,1)S(1)}, bf16[1152,256]{1,0:T(8,128)(2,1)S(1)}, u32[]{:S(2)}, u32[]{:S(2)}) collective-permute-start(bf16[1152,256]{1,0:T(8,128)(2,1)S(1)} %fusion), channel_id=1, source_target_pairs={{1,0},{2,1},{3,2},{0,3},{5,4},{6,5},{7,6},{4,7},{9,8},{10,9},{11,1... | collective-permute-start | bytes 1769480 | tf_op jit(solution)/shard_map/ppermute | solution.py:30
  240.4 10.9 %collective-permute-done = bf16[1152,256]{1,0:T(8,128)(2,1)S(1)} collective-permute-done((bf16[1152,256]{1,0:T(8,128)(2,1)S(1)}, bf16[1152,256]{1,0:T(8,128)(2,1)S(1)}, u32[]{:S(2)}, u32[]{:S(2)}) %collective-permute-start) | collective-permute-done | bytes 589856 | tf_op jit(solution)/shard_map/ppermute | solution.py:25
  251.3 1.9 collective-permute-start.1
  253.3 15.2 %collective-permute-done.1 = bf16[1152,256]{1,0:T(8,128)(2,1)S(1)} collective-permute-done((bf16[1152,256]{1,0:T(8,128)(2,1)S(1)}, bf16[1152,256]{1,0:T(8,128)(2,1)S(1)}, u32[]{:S(2)}, u32[]{:S(2)}) %collective-permute-start.1) | collective-permute-done | bytes 589856 | tf_op jit(solution)/shard_map/ppermute | solution.py:25
  268.5 0.8 copy-done.4
  269.3 1.9 pad_maximum_fusion
  271.2 2.1 gather_fusion
  273.3 3.0 copy.37
  276.3 2.4 convolution_convert_fusion
  278.8 5.3 %all-to-all-start.3 = ((bf16[8,144,512]{2,1,0:T(8,128)(2,1)}), bf16[8,144,512]{2,1,0:T(8,128)(2,1)S(1)}, u32[]{:S(2)}, u32[]{:S(2)}) async-start(bf16[8,144,512]{2,1,0:T(8,128)(2,1)} %bitcast.60), calls=%async_computation.3 | async-start | bytes 2359296 | tf_op jit(solution)/shard_map/all_to_all | solution.py:106
  284.0 25.9 %all-to-all-done.3 = bf16[8,144,512]{2,1,0:T(8,128)(2,1)S(1)} async-done(((bf16[8,144,512]{2,1,0:T(8,128)(2,1)}), bf16[8,144,512]{2,1,0:T(8,128)(2,1)S(1)}, u32[]{:S(2)}, u32[]{:S(2)}) %all-to-all-start.3) | async-done | bytes 1179680 | tf_op jit(solution)/shard_map/all_to_all | solution.py:106
  309.9 0.7 fusion.7
  310.7 0.7 fusion.8
  311.4 72.3 %all_to_all.26 = bf16[8,48,512]{2,1,0:T(8,128)(2,1)S(1)} all-to-all(bf16[8,48,512]{2,1,0:T(8,128)(2,1)S(1)} %bitcast.67), channel_id=1, replica_groups=mesh['grp'=2,'g'=8,'e'=8,'tp'=4] {'g'}, dimensions={0} | all-to-all | bytes 786432 | tf_op jit(solution)/shard_map/all_to_all | solution.py:114
  383.7 1.2 convolution_convert_fusion.2
  (37 shorter events, 0.6 us)
Async XLA Ops:
  6.5 269.8 %copy-start = (bf16[1,1024,512]{2,1,0:T(8,128)(2,1)S(1)}, bf16[1,1024,512]{2,1,0:T(8,128)(2,1)}, u32[]{:S(2)}) copy-start(bf16[1,1024,512]{2,1,0:T(8,128)(2,1)} %param.17) | copy-start | bytes 3145732
  13.2 64.8 %all-to-all-start = ((f32[8,1,192]{2,1,0:T(1,128)}), f32[8,1,192]{2,1,0:T(1,128)S(1)}, u32[]{:S(2)}, u32[]{:S(2)}) async-start(f32[8,1,192]{2,1,0:T(1,128)} %reshape.153), calls=%async_computation | async-start | bytes 16384 | tf_op jit(solution)/shard_map/all_to_all | solution.py:81
  77.9 55.6 %all-to-all-start.1 = ((bf16[8,48,512]{2,1,0:T(8,128)(2,1)}), bf16[8,48,512]{2,1,0:T(8,128)(2,1)S(1)}, u32[]{:S(2)}, u32[]{:S(2)}) async-start(bf16[8,48,512]{2,1,0:T(8,128)(2,1)} %bitcast.3), calls=%async_computation.1 | async-start | bytes 786432 | tf_op jit(solution)/shard_map/all_to_all | solution.py:78
  92.9 134.8 %all-gather.4.cloned.1.call-start = ((), (), s32[]{:S(2)}) async-start(), calls=%async_computation.5 | async-start | bytes 5898240 | tf_op jit(solution)/shard_map/all_gather | solution.py:100
  134.3 93.4 %copy-start.6 = (bf16[1,2048,256]{2,1,0:T(8,128)(2,1)S(1)}, bf16[1,2048,256]{2,1,0:T(8,128)(2,1)}, u32[]{:S(2)}) copy-start(bf16[1,2048,256]{2,1,0:T(8,128)(2,1)} %param.15) | copy-start | bytes 3145732
  175.1 56.6 %copy-start.7 = (bf16[1,2048,256]{2,1,0:T(8,128)(2,1)S(1)}, bf16[1,2048,256]{2,1,0:T(8,128)(2,1)}, u32[]{:S(2)}) copy-start(bf16[1,2048,256]{2,1,0:T(8,128)(2,1)} %param.16) | copy-start | bytes 3145732
  227.8 3.9 copy-start.5
  233.2 35.2 %copy-start.1 = (bf16[1152,256]{1,0:T(8,128)(2,1)}, bf16[1152,256]{1,0:T(8,128)(2,1)S(1)}, u32[]{:S(2)}) copy-start(bf16[1152,256]{1,0:T(8,128)(2,1)S(1)} %fusion) | copy-start | bytes 1769476
  233.2 18.0 %collective-permute-start = (bf16[1152,256]{1,0:T(8,128)(2,1)S(1)}, bf16[1152,256]{1,0:T(8,128)(2,1)S(1)}, u32[]{:S(2)}, u32[]{:S(2)}) collective-permute-start(bf16[1152,256]{1,0:T(8,128)(2,1)S(1)} %fusion), channel_id=1, source_target_pairs={{0,1},{1,2},{2,3},{3,0},{4,5},{5,6},{6,7},{7,4},{8,9},{9,10},{10,1... | collective-permute-start | bytes 1769480 | tf_op jit(solution)/shard_map/ppermute | solution.py:25
  236.1 17.2 %collective-permute-start.2 = (bf16[1152,256]{1,0:T(8,128)(2,1)S(1)}, bf16[1152,256]{1,0:T(8,128)(2,1)S(1)}, u32[]{:S(2)}, u32[]{:S(2)}) collective-permute-start(bf16[1152,256]{1,0:T(8,128)(2,1)S(1)} %fusion), channel_id=1, source_target_pairs={{1,0},{2,1},{3,2},{0,3},{5,4},{6,5},{7,6},{4,7},{9,8},{10,9},{11,1... | collective-permute-start | bytes 1769480 | tf_op jit(solution)/shard_map/ppermute | solution.py:30
  251.3 17.2 %copy-start.2 = (bf16[1152,256]{1,0:T(8,128)(2,1)}, bf16[1152,256]{1,0:T(8,128)(2,1)S(1)}, u32[]{:S(2)}) copy-start(bf16[1152,256]{1,0:T(8,128)(2,1)S(1)} %collective-permute-done) | copy-start | bytes 1769476
  251.3 17.2 %collective-permute-start.1 = (bf16[1152,256]{1,0:T(8,128)(2,1)S(1)}, bf16[1152,256]{1,0:T(8,128)(2,1)S(1)}, u32[]{:S(2)}, u32[]{:S(2)}) collective-permute-start(bf16[1152,256]{1,0:T(8,128)(2,1)S(1)} %collective-permute-done), channel_id=1, source_target_pairs={{0,1},{1,2},{2,3},{3,0},{4,5},{5,6},{6,7},{7,4},{8,9},{9,10},{10,1... | collective-permute-start | bytes 1769480 | tf_op jit(solution)/shard_map/ppermute | solution.py:25
  253.3 15.2 %copy-start.3 = (bf16[1152,256]{1,0:T(8,128)(2,1)}, bf16[1152,256]{1,0:T(8,128)(2,1)S(1)}, u32[]{:S(2)}) copy-start(bf16[1152,256]{1,0:T(8,128)(2,1)S(1)} %collective-permute-done.2) | copy-start | bytes 1769476
  268.5 0.8 copy-start.4
  278.8 31.2 %all-to-all-start.3 = ((bf16[8,144,512]{2,1,0:T(8,128)(2,1)}), bf16[8,144,512]{2,1,0:T(8,128)(2,1)S(1)}, u32[]{:S(2)}, u32[]{:S(2)}) async-start(bf16[8,144,512]{2,1,0:T(8,128)(2,1)} %bitcast.60), calls=%async_computation.3 | async-start | bytes 2359296 | tf_op jit(solution)/shard_map/all_to_all | solution.py:106
Sparse Core Ops, SparseCore 0:
  175.2 52.4 all-gather.3
